TPU v7x, 32 devices: a whole 2x2x4 slice. The times are simulated.
32 devices in a mesh: fs: 16 (over z, y, x), tp: 2 (over core).
Axes of the slice: x: 2, y: 2, z: 4, core: 2. Of those that a mesh axis runs over, the one named last changes fastest.
Arguments:
- tokens: bfloat16 [4096, 2048], P('fs'), may hold values from -6 to 6
- mix_gain: float32 [2048], replicated, may hold values from 0.1 to 1.9
- glu_value: bfloat16 [2048, 2048], P('fs', 'tp'), may hold values from -0.125 to 0.125
- glu_gate: bfloat16 [2048, 2048], P('fs', 'tp'), may hold values from -0.125 to 0.125
- conv_taps: float32 [31, 2048], P(None, 'tp'), may hold values from -2.2 to 2.2, as said below
- chan_gain: float32 [2048], P('tp'), may hold values from 0.1 to 1.9
- mix_out: bfloat16 [2048, 2048], P('tp', 'fs'), may hold values from -0.125 to 0.125
- mlp_gain: float32 [2048], replicated, may hold values from 0.1 to 1.9
- up_weight: bfloat16 [2048, 8192], P('fs', 'tp'), may hold values from -0.125 to 0.125
- down_weight: bfloat16 [8192, 2048], P('tp', 'fs'), may hold values from -0.0625 to 0.0625
Outputs:
- result: bfloat16 [4096, 2048], P('fs')
Inputs may be any that keep to these rules, and one draw needn't show every extreme that they name: `conv_taps`: independent entries scaled by fan-in; channels fall into 16 groups of different scale.
All inputs are finite; a program needn't handle non-finite values.
Results may differ from a plain program's by a relative error of at most 0.018.
Values may be sent and summed in bfloat16 or wider, within the bound.
A program may use at most 128 MiB of HBM per device.

v0:
```python
import functools

import jax
import jax.numpy as jnp
from jax import lax
from jax.experimental import pallas as pl
from jax.experimental.pallas import tpu as pltpu
from jax.sharding import PartitionSpec as P

C = 2048
LEN = 128


norm_floor = 0.05


def rms_scale(stream, gain):
    return stream * lax.rsqrt(jnp.mean(stream * stream, axis=-1, keepdims=True) + norm_floor) * gain


def bf16_round(value):
    return lax.optimization_barrier(value.astype(jnp.bfloat16)).astype(jnp.float32)


def depthwise(glu, conv_taps):
    seqs = glu.shape[0] // LEN
    blocks = glu.reshape(seqs, LEN, glu.shape[1]).astype(jnp.float32)
    reach = conv_taps.shape[0] // 2
    padded = jnp.pad(blocks, ((0, 0), (reach, reach), (0, 0)))
    total = jnp.zeros_like(blocks)
    for offset in range(conv_taps.shape[0]):
        total = total + padded[:, offset : offset + LEN] * conv_taps[offset]
    return total.reshape(glu.shape)


def swap_then_gather(weight, inner, outer, split, join):
    own = lax.all_to_all(
        weight, "fs", split_axis=split, concat_axis=join, axis_index_groups=inner, tiled=True
    )
    return lax.all_gather(own, "fs", axis=join, axis_index_groups=outer, tiled=True)


def shared_sum(partial, inner, tp):
    part = lax.all_to_all(
        partial, "fs", split_axis=0, concat_axis=0, axis_index_groups=inner, tiled=True
    )
    group = len(inner[0])
    rows = partial.shape[0] // group
    part = part.reshape(group, tp, rows // tp, -1).transpose(1, 0, 2, 3)
    part = lax.all_to_all(part, "tp", split_axis=0, concat_axis=0, tiled=True)
    return bf16_round(jnp.sum(part.astype(jnp.float32), axis=(0, 1)))


def plain_device(
    tokens,
    mix_gain,
    glu_value,
    glu_gate,
    conv_taps,
    chan_gain,
    mix_out,
    mlp_gain,
    up_weight,
    down_weight,
):
    fs, tp = lax.axis_size("fs"), lax.axis_size("tp")
    group = 4 if fs % 4 == 0 else 1
    inner = [[o * group + i for i in range(group)] for o in range(fs // group)]
    outer = [[o * group + i for o in range(fs // group)] for i in range(group)]
    place = lax.rem(lax.axis_index("fs"), group)

    value_w = swap_then_gather(glu_value, inner, outer, 1, 0)
    gate_w = swap_then_gather(glu_gate, inner, outer, 1, 0)
    mix_w = swap_then_gather(mix_out, inner, outer, 0, 1)
    up_w = swap_then_gather(up_weight, inner, outer, 1, 0)
    down_w = swap_then_gather(down_weight, inner, outer, 0, 1)

    stream = tokens.astype(jnp.float32)
    normed = rms_scale(stream, mix_gain).astype(jnp.bfloat16)
    normed = lax.all_gather(normed, "fs", axis=0, axis_index_groups=inner, tiled=True)
    values = jnp.dot(normed, value_w, preferred_element_type=jnp.float32)
    gating = jnp.dot(normed, gate_w, preferred_element_type=jnp.float32)
    glu = (values * jax.nn.sigmoid(gating)).astype(jnp.bfloat16)
    channels = value_w.shape[1]
    taps = lax.dynamic_slice_in_dim(conv_taps, place * channels, channels, 1)
    gain = lax.dynamic_slice_in_dim(chan_gain, place * channels, channels, 0)
    convolved = depthwise(glu, taps)
    both = jnp.stack(
        (jnp.sum(convolved, axis=-1), jnp.sum(convolved * convolved, axis=-1))
    )
    both = jnp.sum(lax.all_gather(both, "fs", axis=0, axis_index_groups=inner), axis=0)
    both = lax.psum(both, "tp")
    centre = (both[0] / C)[:, None]
    spread = (both[1] / C)[:, None] - centre * centre
    hidden = jax.nn.silu((convolved - centre) * lax.rsqrt(spread + norm_floor) * gain).astype(
        jnp.bfloat16
    )
    mixed = shared_sum(
        jnp.dot(hidden, mix_w, preferred_element_type=jnp.float32).astype(jnp.bfloat16), inner, tp
    )
    own_rows = stream.shape[0] // tp
    own_stream = lax.dynamic_slice_in_dim(stream, lax.axis_index("tp") * own_rows, own_rows, 0)
    resid = own_stream + mixed
    normed_mlp = rms_scale(resid, mlp_gain).astype(jnp.bfloat16)
    normed_mlp = lax.all_gather(normed_mlp, "fs", axis=0, axis_index_groups=inner)
    normed_mlp = lax.all_gather(normed_mlp, "tp", axis=1).reshape(-1, normed.shape[1])
    active = jnp.square(
        jax.nn.relu(jnp.dot(normed_mlp, up_w, preferred_element_type=jnp.float32))
    ).astype(jnp.bfloat16)
    feed = shared_sum(
        jnp.dot(active, down_w, preferred_element_type=jnp.float32).astype(jnp.bfloat16), inner, tp
    )
    finished = (resid + feed).astype(jnp.bfloat16)
    return lax.all_gather(finished, "tp", axis=0, tiled=True)

MESH = pl.DeviceIdType.MESH
F32, BF16 = jnp.float32, jnp.bfloat16


def rows_at(start, size):
    return pl.ds(pl.multiple_of(start, 128), size)


def layer_kernel(
    ng,
    tok, mixg, gv, gg, taps, chg, mo, mlpg, up, dn,
    out,
    fgv, fgg, fmo, fup, fdn,
    tok_all, nrm, pad, cv, hid, st, st_all,
    acc, resid, nm_all, act, fin,
    sbo1, sbi1, rdo1, rdi1, sbo2, sbi2, rdo2, rdi2,
    ws, wr, lsem, tsem, nsem, ssem, rsem, fsem,
):
    f, t = lax.axis_index("fs"), lax.axis_index("tp")
    x, y = lax.rem(f, 2), lax.rem(lax.div(f, 2), 2)
    zp, zh = lax.rem(lax.div(f, 4), 2), lax.div(f, 8)
    sib = 1 - t
    L = tok.shape[0] // 2
    half = ng * L
    width = tok.shape[1]
    chans = fgv.shape[1]
    hidden = fup.shape[1]
    depth = gv.shape[0]
    sends = []

    def flip(coord, bit):
        return 1 - coord if bit else coord

    def chip(dq):
        return flip(zp, dq // 2) * 2 + flip(x, dq % 2)

    def fs_of(dq, do):
        return flip(zh, do // 2) * 8 + flip(zp, dq // 2) * 4 + flip(y, do % 2) * 2 + flip(x, dq % 2)

    p = chip(0)

    def push(src, dst, s_sem, r_sem, device):
        copy = pltpu.make_async_remote_copy(
            src_ref=src, dst_ref=dst, send_sem=s_sem, recv_sem=r_sem,
            device_id=device, device_id_type=MESH,
        )
        copy.start()
        sends.append(copy)

    def arrived(dst, s_sem, r_sem):
        pltpu.make_async_remote_copy(
            src_ref=dst, dst_ref=dst, send_sem=s_sem, recv_sem=r_sem,
            device_id=(f, sib), device_id_type=MESH,
        ).wait_recv()

    barrier = pltpu.get_barrier_semaphore()
    peers = [(fs_of(dq, 0), u) for dq in range(1, ng) for u in (t, sib)]
    peers += [(f, sib), (fs_of(0, 1), t), (fs_of(0, 2), t)]
    for peer in peers:
        pl.semaphore_signal(barrier, inc=1, device_id=peer, device_id_type=MESH)
    pl.semaphore_wait(barrier, len(peers))

    weights = (
        (lambda q: gv.at[:, rows_at(q * chans, chans)], lambda g: fgv.at[rows_at(g * depth, depth), :]),
        (lambda q: gg.at[:, rows_at(q * chans, chans)], lambda g: fgg.at[rows_at(g * depth, depth), :]),
        (lambda q: mo.at[rows_at(q * chans, chans), :], lambda g: fmo.at[:, rows_at(g * depth, depth)]),
        (lambda q: up.at[:, rows_at(q * hidden, hidden)], lambda g: fup.at[rows_at(g * depth, depth), :]),
        (lambda q: dn.at[rows_at(q * hidden, hidden), :], lambda g: fdn.at[:, rows_at(g * depth, depth)]),
    )

    def spread_in_plane(a):
        src, dst = weights[a]
        for dq in range(1, ng):
            push(src(chip(dq)), dst(f), ws.at[a, dq], wr.at[a, dq], (fs_of(dq, 0), t))

    def spread_own(a):
        src, dst = weights[a]
        for do in (2, 1):
            push(src(p), dst(f), ws.at[a, do * ng], wr.at[a, do * ng], (fs_of(0, do), t))

    def forward(a):
        dst = weights[a][1]
        for dq in range(1, ng):
            piece = dst(fs_of(dq, 0))
            arrived(piece, ws.at[a, 0], wr.at[a, dq])
            for do in (2, 1):
                push(piece, piece, ws.at[a, do * ng + dq], wr.at[a, do * ng + dq], (fs_of(0, do), t))

    def relay(a, which=(0, 1, 2, 3)):
        dst = weights[a][1]
        for dq in which:
            piece = dst(fs_of(dq, 2))
            arrived(piece, ws.at[a, 0], wr.at[a, 2 * ng + dq])
            push(piece, piece, ws.at[a, 3 * ng + dq], wr.at[a, 3 * ng + dq], (fs_of(0, 1), t))

    def whole(a):
        dst = weights[a][1]
        for do in (1, 3):
            for dq in range(ng):
                arrived(dst(fs_of(dq, do)), ws.at[a, 0], wr.at[a, do * ng + dq])
        local(a).wait()

    def local(a):
        src, dst = weights[a]
        return pltpu.make_async_copy(src(p), dst(f), lsem.at[a])

    for a in (0, 1):
        spread_in_plane(a)
    for a in (0, 1):
        spread_own(a)
    for dq in range(1, ng):
        push(
            tok.at[rows_at(t * L, L)], tok_all.at[rows_at(t * half + p * L, L)],
            tsem.at[0, dq], tsem.at[1, dq], (fs_of(dq, 0), t),
        )
    spread_in_plane(2)
    spread_own(2)
    for a in (3, 4):
        spread_in_plane(a)
    for a in range(5):
        local(a).start()

    step = 16

    def norm_rows(load, gain, dst, start):
        def body(i, _):
            value = load(i * step).astype(F32)
            scale = lax.rsqrt(jnp.mean(value * value, axis=-1, keepdims=True) + norm_floor)
            dst[pl.ds(pl.multiple_of(start + i * step, step), step), :] = (
                value * scale * gain[...]
            ).astype(BF16)
            return 0

        lax.fori_loop(0, L // step, body, 0)

    def from_ref(ref, base):
        return lambda i: ref[pl.ds(pl.multiple_of(base + i, step), step), :]

    for u in range(2):
        norm_rows(from_ref(tok, u * L), mixg, nrm, u * half + p * L)
    for a in (0, 1):
        forward(a)
    for dq in range(1, ng):
        block = tok_all.at[rows_at(t * half + chip(dq) * L, L)]
        arrived(block, tsem.at[0, 0], tsem.at[1, dq])
        push(block, block, tsem.at[2, dq], tsem.at[3, dq], (f, sib))
        norm_rows(from_ref(tok_all, t * half + chip(dq) * L), mixg, nrm, t * half + chip(dq) * L)
    forward(2)
    for a in (3, 4):
        spread_own(a)
    for dq in range(1, ng):
        start = sib * half + chip(dq) * L
        arrived(tok_all.at[rows_at(start, L)], tsem.at[0, 0], tsem.at[3, dq])
        norm_rows(from_ref(tok_all, start), mixg, nrm, start)

    relay(0)
    relay(1)
    whole(0)
    whole(1)
    pad[...] = jnp.zeros_like(pad)
    st[...] = jnp.zeros_like(st)
    taps_n = taps.shape[0]
    reach = taps_n // 2
    lead = (reach + 7) // 8 * 8
    own_cols = p * chans
    eye = lax.broadcasted_iota(jnp.int32, (L, L), 0) == lax.broadcasted_iota(jnp.int32, (L, L), 1)

    def conv_block(b, _):
        rows = rows_at(b * L, L)
        left = nrm[rows, :]
        values = jnp.dot(left, fgv[...], preferred_element_type=F32)
        gating = jnp.dot(left, fgg[...], preferred_element_type=F32)
        glu = (values * jax.nn.sigmoid(gating)).astype(BF16).astype(F32)
        pad[pl.ds(lead, L), :] = glu
        sums = jnp.zeros((L, 1), F32)
        squares = jnp.zeros((L, 1), F32)
        for c in range(chans // 128):
            total = jnp.zeros((L, 128), F32)
            for j in range(taps_n):
                tap = taps[pl.ds(j, 1), rows_at(own_cols + c * 128, 128)]
                total = total + pad[pl.ds(lead - reach + j, L), pl.ds(c * 128, 128)] * tap
            cv[rows, pl.ds(c * 128, 128)] = total
            sums = sums + jnp.sum(total, axis=1, keepdims=True)
            squares = squares + jnp.sum(total * total, axis=1, keepdims=True)
        st[b, pl.ds(0, 1), :] = jnp.sum(jnp.where(eye, sums, 0.0), axis=0, keepdims=True)
        st[b, pl.ds(1, 1), :] = jnp.sum(jnp.where(eye, squares, 0.0), axis=0, keepdims=True)
        return 0

    lax.fori_loop(0, 2 * ng, conv_block, 0)

    slots = [(dq, du) for dq in range(ng) for du in range(2) if (dq, du) != (0, 0)]
    for dq, du in slots:
        push(
            st, st_all.at[dq * 2 + du],
            ssem.at[0, dq * 2 + du], ssem.at[1, dq * 2 + du],
            (fs_of(dq, 0), t if du == 0 else sib),
        )
    forward(3)
    relay(2)
    forward(4)
    for dq, du in slots:
        arrived(st_all.at[dq * 2 + du], ssem.at[0, 0], ssem.at[1, dq * 2 + du])

    def hidden_block(b, _):
        rows = rows_at(b * L, L)
        total = st[b]
        for dq, du in slots:
            total = total + st_all[dq * 2 + du, b]
        count = chans * ng * 2
        sums = jnp.sum(jnp.where(eye, total[0:1, :], 0.0), axis=1, keepdims=True)
        squares = jnp.sum(jnp.where(eye, total[1:2, :], 0.0), axis=1, keepdims=True)
        centre = sums / count
        spread = squares / count - centre * centre
        value = (cv[rows, :] - centre) * lax.rsqrt(spread + norm_floor)
        value = value * chg[:, rows_at(own_cols, chans)]
        hid[rows, :] = (value * jax.nn.sigmoid(value)).astype(BF16)
        return 0

    lax.fori_loop(0, 2 * ng, hidden_block, 0)

    cols = 512

    def reduce_rows(left, right, sbo, sbi, rdo, rdi, k):
        def theirs(n, _):
            at = rows_at(n * cols, cols)
            sbo[:, at] = jnp.dot(
                left[rows_at(sib * half, half), :], right[:, at], preferred_element_type=F32
            ).astype(BF16)
            return 0

        lax.fori_loop(0, width // cols, theirs, 0)
        push(sbo, sbi, rsem.at[k, 0], rsem.at[k, 1], (f, sib))

        def mine(n, _):
            at = rows_at(n * cols, cols)
            acc[:, at] = jnp.dot(
                left[rows_at(t * half, half), :], right[:, at], preferred_element_type=F32
            )
            return 0

        lax.fori_loop(0, width // cols, mine, 0)
        arrived(sbi, rsem.at[k, 0], rsem.at[k, 1])
        for dq in range(1, ng):
            base = chip(dq) * L

            def add(i, _):
                at = pl.ds(pl.multiple_of(base + i * step, step), step)
                rdo[at, :] = (acc[at, :] + sbi[at, :].astype(F32)).astype(BF16)
                return 0

            lax.fori_loop(0, L // step, add, 0)
            push(
                rdo.at[rows_at(base, L)], rdi.at[dq - 1],
                rsem.at[k, 2 * dq], rsem.at[k, 2 * dq + 1], (fs_of(dq, 0), t),
            )

    def reduced(sbi, rdi, i):
        at = pl.ds(pl.multiple_of(p * L + i * step, step), step)
        total = acc[at, :] + sbi[at, :].astype(F32)
        for dq in range(1, ng):
            total = total + rdi[dq - 1, pl.ds(pl.multiple_of(i * step, step), step), :].astype(F32)
        return total.astype(BF16).astype(F32)

    def wait_reduced(rdi, k):
        for dq in range(1, ng):
            arrived(rdi.at[dq - 1], rsem.at[k, 0], rsem.at[k, 2 * dq + 1])

    whole(2)
    reduce_rows(hid, fmo, sbo1, sbi1, rdo1, rdi1, 0)
    wait_reduced(rdi1, 0)

    def resid_rows(i, _):
        at = pl.ds(pl.multiple_of(i * step, step), step)
        own = tok[pl.ds(pl.multiple_of(t * L + i * step, step), step), :].astype(F32)
        value = own + reduced(sbi1, rdi1, i)
        resid[at, :] = value
        scale = lax.rsqrt(jnp.mean(value * value, axis=-1, keepdims=True) + norm_floor)
        nm_all[pl.ds(pl.multiple_of(t * half + p * L + i * step, step), step), :] = (
            value * scale * mlpg[...]
        ).astype(BF16)
        return 0

    lax.fori_loop(0, L // step, resid_rows, 0)
    mine = nm_all.at[rows_at(t * half + p * L, L)]
    for dq in range(1, ng):
        push(mine, mine, nsem.at[0, dq], nsem.at[1, dq], (fs_of(dq, 0), t))
    push(mine, mine, nsem.at[2, 0], nsem.at[3, 0], (f, sib))
    relay(3)
    for dq in range(1, ng):
        block = nm_all.at[rows_at(t * half + chip(dq) * L, L)]
        arrived(block, nsem.at[0, 0], nsem.at[1, dq])
        push(block, block, nsem.at[2, dq], nsem.at[3, dq], (f, sib))

    whole(3)

    def up_half(u):
        def body(n, _):
            at = rows_at(n * 256, 256)
            value = jnp.dot(
                nm_all[rows_at(u * half, half), :], fup[:, at], preferred_element_type=F32
            )
            value = jnp.maximum(value, 0.0)
            act[rows_at(u * half, half), at] = (value * value).astype(BF16)
            return 0

        lax.fori_loop(0, hidden // 256, body, 0)

    up_half(t)
    relay(4, (0, 1))
    for dq in range(ng):
        arrived(nm_all.at[rows_at(sib * half + chip(dq) * L, L)], nsem.at[0, 0], nsem.at[3, dq])
    up_half(sib)
    relay(4, (2, 3))
    whole(4)
    reduce_rows(act, fdn, sbo2, sbi2, rdo2, rdi2, 1)
    wait_reduced(rdi2, 1)

    def finish_rows(i, _):
        at = pl.ds(pl.multiple_of(i * step, step), step)
        value = (resid[at, :] + reduced(sbi2, rdi2, i)).astype(BF16)
        fin[0, at, :] = value
        out[pl.ds(pl.multiple_of(t * L + i * step, step), step), :] = value
        return 0

    lax.fori_loop(0, L // step, finish_rows, 0)
    push(fin.at[0], fin.at[1], fsem.at[0], fsem.at[1], (f, sib))
    arrived(fin.at[1], fsem.at[0], fsem.at[1])

    def copy_rows(i, _):
        at = pl.ds(pl.multiple_of(i * step, step), step)
        out[pl.ds(pl.multiple_of(sib * L + i * step, step), step), :] = fin[1, at, :]
        return 0

    lax.fori_loop(0, L // step, copy_rows, 0)
    for copy in sends:
        copy.wait_send()


def fused_device(ng, nz, tokens, mix_gain, glu_value, glu_gate, conv_taps, chan_gain, mix_out, mlp_gain, up_weight, down_weight):
    rows, width = tokens.shape
    fs = ng * nz
    L = rows // 2
    half = ng * L
    chans = glu_value.shape[1] // ng
    hidden = up_weight.shape[1] // ng
    depth = glu_value.shape[0]
    blocks = 2 * ng
    vm = pltpu.VMEM
    dma = pltpu.SemaphoreType.DMA
    reduce_bufs = [
        vm((half, width), BF16), vm((half, width), BF16), vm((half, width), BF16),
        vm((ng - 1, L, width), BF16),
    ]
    scratch = [
        vm((fs * depth, chans), BF16), vm((fs * depth, chans), BF16), vm((chans, width), BF16),
        vm((fs * depth, hidden), BF16), vm((hidden, width), BF16),
        vm((2 * half, width), BF16), vm((2 * half, width), BF16),
        vm((L + 32, chans), F32), vm((2 * half, chans), F32), vm((2 * half, chans), BF16),
        vm((blocks, 8, L), F32), vm((blocks, blocks, 8, L), F32),
        vm((half, width), F32), vm((L, width), F32), vm((2 * half, width), BF16),
        vm((2 * half, hidden), BF16), vm((2, L, width), BF16),
        *reduce_bufs, *reduce_bufs,
        dma((5, fs)), dma((5, fs)), dma((5,)), dma((4, ng)), dma((4, ng)),
        dma((2, blocks)), dma((2, 2 * ng)), dma((2,)),
    ]
    return pl.pallas_call(
        functools.partial(layer_kernel, ng),
        out_shape=jax.ShapeDtypeStruct((rows, width), BF16),
        in_specs=[pl.BlockSpec(memory_space=vm)] * 10,
        out_specs=pl.BlockSpec(memory_space=vm),
        scratch_shapes=scratch,
        compiler_params=pltpu.CompilerParams(
            collective_id=0, has_side_effects=True, vmem_limit_bytes=60 * 1024 * 1024
        ),
    )(
        tokens, mix_gain[None], glu_value, glu_gate, conv_taps, chan_gain[None], mix_out,
        mlp_gain[None], up_weight, down_weight,
    )


def per_device(*args):
    tokens, glu_value, conv_taps = args[0], args[2], args[4]
    fs, tp = lax.axis_size("fs"), lax.axis_size("tp")
    group = 4
    fits = (
        tp == 2
        and fs == group * 4
        and tokens.shape[0] == 2 * LEN
        and glu_value.shape[0] % 128 == 0
        and conv_taps.shape[1] % (group * 128) == 0
        and conv_taps.shape[0] <= 31
    )
    if fits:
        return fused_device(group, fs // group, *args)
    return plain_device(*args)


def solution(mesh):
    in_specs = (
        P("fs", None),
        P(),
        P("fs", "tp"),
        P("fs", "tp"),
        P(None, "tp"),
        P("tp"),
        P("tp", "fs"),
        P(),
        P("fs", "tp"),
        P("tp", "fs"),
    )
    out_specs = P("fs", None)
    return jax.shard_map(
        per_device, mesh=mesh, in_specs=in_specs, out_specs=out_specs, check_vma=False
    )
```

profile of v0, /device:TPU:0, one launch (start us, length us, event | category | flops | bytes accessed | tf_op | source)
XLA Modules:
  0.0 252.2 jit_solution(17701521116738053665)
XLA Ops:
  0.0 249.9 %shard_map.100 = bf16[256,2048]{1,0:T(8,128)(2,1)} custom-call(bf16[256,2048]{1,0:T(8,128)(2,1)} %tok.1, f32[1,2048]{1,0:T(1,128)} %bitcast.3, bf16[128,1024]{1,0:T(8,128)(2,1)} %gv.1, bf16[128,1024]{1,0:T(8,128)(2,1)} %gg.1, f32[31,1024]{1,0:T(8,128)} %taps.1, f32[1,1024]{1,0:T(1,128)} %bitcast.5, bf16[1024,128]{1,0:T(8,128)(2,1)} %mo.1, ...), custom_call_target="tpu_custom_call" | custom-call | tf_op jit(solution)/shard_map/pallas_call | solution.py:481
  249.9 2.3 copy.12
where the time goes:
time: 252 us
  Pallas kernels  250 us (99%)
    pallas_call x1, Pallas kernels, fused_device(): pl.pallas_call(functools.partial(layer_kernel, ng), out_shape=jax.ShapeDt...  250 us

commit v1 on v0

--- a/solution.py
+++ b/solution.py
@@ -126,7 +126,7 @@
     tok, mixg, gv, gg, taps, chg, mo, mlpg, up, dn,
     out,
     fgv, fgg, fmo, fup, fdn,
-    tok_all, nrm, pad, cv, hid, st, st_all,
+    nrm, pad, cv, hid, st, st_all,
     acc, resid, nm_all, act, fin,
     sbo1, sbi1, rdo1, rdi1, sbo2, sbi2, rdo2, rdi2,
     ws, wr, lsem, tsem, nsem, ssem, rsem, fsem,
@@ -134,6 +134,7 @@
     f, t = lax.axis_index("fs"), lax.axis_index("tp")
     x, y = lax.rem(f, 2), lax.rem(lax.div(f, 2), 2)
     zp, zh = lax.rem(lax.div(f, 4), 2), lax.div(f, 8)
+    mid = lax.rem(zp + zh, 2)
     sib = 1 - t
     L = tok.shape[0] // 2
     half = ng * L
@@ -141,36 +142,61 @@
     chans = fgv.shape[1]
     hidden = fup.shape[1]
     depth = gv.shape[0]
-    sends = []
+    sends, sent = [], set()
 
     def flip(coord, bit):
         return 1 - coord if bit else coord
 
     def chip(dq):
-        return flip(zp, dq // 2) * 2 + flip(x, dq % 2)
+        return flip(mid, dq // 2) * 2 + flip(x, dq % 2)
 
     def fs_of(dq, do):
-        return flip(zh, do // 2) * 8 + flip(zp, dq // 2) * 4 + flip(y, do % 2) * 2 + flip(x, dq % 2)
-
-    p = chip(0)
-
-    def push(src, dst, s_sem, r_sem, device):
-        copy = pltpu.make_async_remote_copy(
+        return flip(zh, do // 2) * 8 + flip(zp, (dq // 2 + do // 2) % 2) * 4 + flip(y, do % 2) * 2 + flip(x, dq % 2)
+
+    def seat(dq):
+        return flip(y, dq // 2) * 2 + flip(x, dq % 2)
+
+    def seat_fs(dq, do=0):
+        return zh * 8 + zp * 4 + flip(y, dq // 2) * 2 + flip(x, dq % 2)
+
+    p, s = chip(0), seat(0)
+    near, mate = fs_of(2, 0), fs_of(0, 2)
+    z = zh * 2 + zp
+    z_near = zh * 2 + 1 - zp
+    z_mate, z_far = (1 - zh) * 2 + zh, (1 - zh) * 2 + 1 - zh
+    outer, inner = mid == 0, mid == 1
+
+    def remote(src, dst, s_sem, r_sem, device):
+        return pltpu.make_async_remote_copy(
             src_ref=src, dst_ref=dst, send_sem=s_sem, recv_sem=r_sem,
             device_id=device, device_id_type=MESH,
         )
-        copy.start()
-        sends.append(copy)
+
+    def act_if(when, act):
+        if when is None:
+            act()
+        else:
+            pl.when(when)(act)
+
+    def start(src, dst, s_sem, r_sem, device, when=None):
+        copy = remote(src, dst, s_sem, r_sem, device)
+        act_if(when, copy.start)
+        return copy
+
+    def push(src, dst, s_sem, r_sem, device, when=None):
+        sends.append((start(src, dst, s_sem, r_sem, device, when), when))
+
+    def once(key, copy):
+        if key not in sent:
+            sent.add(key)
+            sends.append((copy, None))
 
     def arrived(dst, s_sem, r_sem):
-        pltpu.make_async_remote_copy(
-            src_ref=dst, dst_ref=dst, send_sem=s_sem, recv_sem=r_sem,
-            device_id=(f, sib), device_id_type=MESH,
-        ).wait_recv()
+        remote(dst, dst, s_sem, r_sem, (f, sib)).wait_recv()
 
     barrier = pltpu.get_barrier_semaphore()
-    peers = [(fs_of(dq, 0), u) for dq in range(1, ng) for u in (t, sib)]
-    peers += [(f, sib), (fs_of(0, 1), t), (fs_of(0, 2), t)]
+    peers = [(seat_fs(dq), u) for dq in range(1, ng) for u in (t, sib)]
+    peers += [(f, sib), (near, t), (fs_of(3, 0), t), (mate, t)]
     for peer in peers:
         pl.semaphore_signal(barrier, inc=1, device_id=peer, device_id_type=MESH)
     pl.semaphore_wait(barrier, len(peers))
@@ -183,30 +209,48 @@
         (lambda q: dn.at[rows_at(q * hidden, hidden), :], lambda g: fdn.at[:, rows_at(g * depth, depth)]),
     )
 
-    def spread_in_plane(a):
+    def spread_in_plane(a, which=(1, 2, 3), when=None):
         src, dst = weights[a]
-        for dq in range(1, ng):
-            push(src(chip(dq)), dst(f), ws.at[a, dq], wr.at[a, dq], (fs_of(dq, 0), t))
-
-    def spread_own(a):
+        part, place = (seat, seat_fs) if a < 3 else (chip, fs_of)
+        for dq in which:
+            copy = start(src(part(dq)), dst(f), ws.at[a, dq], wr.at[a, dq], (place(dq, 0), t), when)
+            once((a, 0, dq), copy)
+
+    def send(a, do, which=(0, 1, 2, 3), when=None):
         src, dst = weights[a]
-        for do in (2, 1):
-            push(src(p), dst(f), ws.at[a, do * ng], wr.at[a, do * ng], (fs_of(0, do), t))
-
-    def forward(a):
-        dst = weights[a][1]
-        for dq in range(1, ng):
+        for dq in which:
             piece = dst(fs_of(dq, 0))
-            arrived(piece, ws.at[a, 0], wr.at[a, dq])
-            for do in (2, 1):
-                push(piece, piece, ws.at[a, do * ng + dq], wr.at[a, do * ng + dq], (fs_of(0, do), t))
-
-    def relay(a, which=(0, 1, 2, 3)):
+            copy = start(
+                src(p) if dq == 0 else piece, piece,
+                ws.at[a, do * ng + dq], wr.at[a, do * ng + dq], (fs_of(0, do), t), when,
+            )
+            once((a, do, dq), copy)
+
+    def got(a, dq, when=None):
+        piece = weights[a][1]((seat_fs if a < 3 else fs_of)(dq, 0))
+        come = remote(piece, piece, ws.at[a, 0], wr.at[a, dq], (f, sib))
+        act_if(when, come.wait_recv)
+
+    def got_and_send(a, which, when=None, zh_when=None):
+        for dq in which:
+            got(a, dq, when)
+            send(a, 1, (dq,), when)
+            if zh_when is not None:
+                send(a, 2, (dq,), zh_when)
+
+    def relay(a, which=(0, 1, 2, 3), when=None):
         dst = weights[a][1]
         for dq in which:
             piece = dst(fs_of(dq, 2))
-            arrived(piece, ws.at[a, 0], wr.at[a, 2 * ng + dq])
-            push(piece, piece, ws.at[a, 3 * ng + dq], wr.at[a, 3 * ng + dq], (fs_of(0, 1), t))
+            come = remote(piece, piece, ws.at[a, 0], wr.at[a, 2 * ng + dq], (f, sib))
+            copy = remote(piece, piece, ws.at[a, 3 * ng + dq], wr.at[a, 3 * ng + dq], (fs_of(0, 1), t))
+
+            def pass_on():
+                come.wait_recv()
+                copy.start()
+
+            act_if(when, pass_on)
+            once((a, 3, dq), copy)
 
     def whole(a):
         dst = weights[a][1]
@@ -217,23 +261,65 @@
 
     def local(a):
         src, dst = weights[a]
-        return pltpu.make_async_copy(src(p), dst(f), lsem.at[a])
-
-    for a in (0, 1):
-        spread_in_plane(a)
-    for a in (0, 1):
-        spread_own(a)
-    for dq in range(1, ng):
-        push(
-            tok.at[rows_at(t * L, L)], tok_all.at[rows_at(t * half + p * L, L)],
-            tsem.at[0, dq], tsem.at[1, dq], (fs_of(dq, 0), t),
-        )
-    spread_in_plane(2)
-    spread_own(2)
-    for a in (3, 4):
-        spread_in_plane(a)
-    for a in range(5):
-        local(a).start()
+        return pltpu.make_async_copy(src(s if a < 3 else p), dst(f), lsem.at[a])
+
+    planes = (
+        lambda g: fgv.at[rows_at(g * ng * depth, ng * depth), :],
+        lambda g: fgg.at[rows_at(g * ng * depth, ng * depth), :],
+        lambda g: fmo.at[:, rows_at(g * ng * depth, ng * depth)],
+    )
+
+    def line(a, g, s_at, r_at, to, when=None):
+        block = planes[a](g)
+        push(block, block, ws.at[a, s_at], wr.at[a, r_at], (to, t), when)
+
+    def line_got(a, g, r_at, when):
+        come = remote(planes[a](g), planes[a](g), ws.at[a, 0], wr.at[a, r_at], (f, sib))
+        act_if(when, come.wait_recv)
+
+    def line_own(a, when=None):
+        line(a, z, 4, 4, near, when)
+        if when is not outer:
+            line(a, z, 7, 5, mate, inner)
+
+    def line_near(a):
+        line_got(a, z_near, 4, inner)
+        line(a, z_near, 8, 6, mate, inner)
+
+    def line_mate(a):
+        line_got(a, z_mate, 5, inner)
+        line(a, z_mate, 5, 5, near, inner)
+
+    def line_far(a):
+        line_got(a, z_far, 6, inner)
+        line(a, z_far, 6, 6, near, inner)
+
+    def line_whole(a):
+        for g, r_at in ((z_near, 4), (z_mate, 5), (z_far, 6)):
+            line_got(a, g, r_at, outer)
+
+    first = (nrm, tsem, seat, seat_fs)
+    second = (nm_all, nsem, chip, fs_of)
+
+    def gather_start(buf, sem, part, place):
+        own = buf.at[rows_at(t * half + part(0) * L, L)]
+        for dq in (2, 1):
+            push(own, own, sem.at[0, dq], sem.at[1, dq], (place(dq, 0), t))
+        push(own, own, sem.at[2, 0], sem.at[3, 0], (f, sib))
+
+    def gather_relay(rows, *which):
+        buf, sem, part, place = rows
+        for dq in which:
+            block = buf.at[rows_at(t * half + part(dq) * L, L)]
+            arrived(block, sem.at[0, 0], sem.at[1, dq])
+            if dq == 2:
+                push(block, block, sem.at[0, 3], sem.at[1, 3], (place(1, 0), t))
+            push(block, block, sem.at[2, dq], sem.at[3, dq], (f, sib))
+
+    def gather_finish(rows, *which):
+        buf, sem, part, place = rows
+        for dq in which:
+            arrived(buf.at[rows_at(sib * half + part(dq) * L, L)], sem.at[0, 0], sem.at[3, dq])
 
     step = 16
 
@@ -251,36 +337,50 @@
     def from_ref(ref, base):
         return lambda i: ref[pl.ds(pl.multiple_of(base + i, step), step), :]
 
-    for u in range(2):
-        norm_rows(from_ref(tok, u * L), mixg, nrm, u * half + p * L)
     for a in (0, 1):
-        forward(a)
-    for dq in range(1, ng):
-        block = tok_all.at[rows_at(t * half + chip(dq) * L, L)]
-        arrived(block, tsem.at[0, 0], tsem.at[1, dq])
-        push(block, block, tsem.at[2, dq], tsem.at[3, dq], (f, sib))
-        norm_rows(from_ref(tok_all, t * half + chip(dq) * L), mixg, nrm, t * half + chip(dq) * L)
-    forward(2)
+        spread_in_plane(a)
+    for a in range(5):
+        local(a).start()
+    norm_rows(from_ref(tok, t * L), mixg, nrm, t * half + s * L)
+    gather_start(*first)
+    spread_in_plane(2)
+
+    def plane_ready(a):
+        for dq in (1, 2, 3):
+            got(a, dq)
+        local(a).wait()
+
+    for a in (0, 1):
+        plane_ready(a)
+        line_own(a)
+    gather_relay(first, 2, 1)
     for a in (3, 4):
-        spread_own(a)
-    for dq in range(1, ng):
-        start = sib * half + chip(dq) * L
-        arrived(tok_all.at[rows_at(start, L)], tsem.at[0, 0], tsem.at[3, dq])
-        norm_rows(from_ref(tok_all, start), mixg, nrm, start)
-
-    relay(0)
-    relay(1)
-    whole(0)
-    whole(1)
+        spread_in_plane(a, (1,))
+        send(a, 1, (0,))
+    for step_of in (line_near, line_mate):
+        for a in (0, 1):
+            step_of(a)
+    plane_ready(2)
+    line_own(2, outer)
+    for a in (0, 1):
+        line_far(a)
+    line_own(2, inner)
+    line_near(2)
+    send(3, 2, (0,), inner)
+    spread_in_plane(3, (3, 2), outer)
+    gather_finish(first, 0, 1)
+    for a in (0, 1):
+        line_whole(a)
     pad[...] = jnp.zeros_like(pad)
     st[...] = jnp.zeros_like(st)
     taps_n = taps.shape[0]
     reach = taps_n // 2
     lead = (reach + 7) // 8 * 8
-    own_cols = p * chans
+    own_cols = s * chans
     eye = lax.broadcasted_iota(jnp.int32, (L, L), 0) == lax.broadcasted_iota(jnp.int32, (L, L), 1)
 
-    def conv_block(b, _):
+    def conv_block(i, _):
+        b = lax.rem(i, 2) * ng + lax.rem(y + lax.div(i, 4), 2) * 2 + lax.rem(x + lax.div(i, 2), 2)
         rows = rows_at(b * L, L)
         left = nrm[rows, :]
         values = jnp.dot(left, fgv[...], preferred_element_type=F32)
@@ -301,18 +401,26 @@
         st[b, pl.ds(1, 1), :] = jnp.sum(jnp.where(eye, squares, 0.0), axis=0, keepdims=True)
         return 0
 
-    lax.fori_loop(0, 2 * ng, conv_block, 0)
+    lax.fori_loop(0, ng, conv_block, 0)
+    gather_relay(first, 3)
+    line_mate(2)
+    got_and_send(3, (1,), None, inner)
+    spread_in_plane(4, (3, 2), outer)
+    gather_finish(first, 2, 3)
+    lax.fori_loop(ng, 2 * ng, conv_block, 0)
 
     slots = [(dq, du) for dq in range(ng) for du in range(2) if (dq, du) != (0, 0)]
     for dq, du in slots:
         push(
             st, st_all.at[dq * 2 + du],
             ssem.at[0, dq * 2 + du], ssem.at[1, dq * 2 + du],
-            (fs_of(dq, 0), t if du == 0 else sib),
+            (seat_fs(dq), t if du == 0 else sib),
         )
-    forward(3)
-    relay(2)
-    forward(4)
+    line_far(2)
+    spread_in_plane(3, (3, 2), inner)
+    spread_in_plane(4, (3, 2), inner)
+    send(4, 2, (0,), inner)
+    got_and_send(4, (1,), None, inner)
     for dq, du in slots:
         arrived(st_all.at[dq * 2 + du], ssem.at[0, 0], ssem.at[1, dq * 2 + du])
 
@@ -335,7 +443,7 @@
 
     cols = 512
 
-    def reduce_rows(left, right, sbo, sbi, rdo, rdi, k):
+    def reduce_rows(left, right, sbo, sbi, rdo, rdi, k, part, place, between=lambda: None):
         def theirs(n, _):
             at = rows_at(n * cols, cols)
             sbo[:, at] = jnp.dot(
@@ -355,39 +463,53 @@
 
         lax.fori_loop(0, width // cols, mine, 0)
         arrived(sbi, rsem.at[k, 0], rsem.at[k, 1])
-        for dq in range(1, ng):
-            base = chip(dq) * L
+        for dq in (3, 1, 2):
+            base = part(dq) * L
+            if dq == 2:
+                between()
+                arrived(rdi.at[2], rsem.at[k, 0], rsem.at[k, 7])
 
             def add(i, _):
                 at = pl.ds(pl.multiple_of(base + i * step, step), step)
-                rdo[at, :] = (acc[at, :] + sbi[at, :].astype(F32)).astype(BF16)
+                total = acc[at, :] + sbi[at, :].astype(F32)
+                if dq == 2:
+                    total = total + rdi[2, pl.ds(pl.multiple_of(i * step, step), step), :].astype(F32)
+                rdo[at, :] = total.astype(BF16)
                 return 0
 
             lax.fori_loop(0, L // step, add, 0)
             push(
                 rdo.at[rows_at(base, L)], rdi.at[dq - 1],
-                rsem.at[k, 2 * dq], rsem.at[k, 2 * dq + 1], (fs_of(dq, 0), t),
+                rsem.at[k, 2 * dq], rsem.at[k, 2 * dq + 1], (place(2 if dq == 2 else 1, 0), t),
             )
 
-    def reduced(sbi, rdi, i):
-        at = pl.ds(pl.multiple_of(p * L + i * step, step), step)
+    def reduced(sbi, rdi, own, i):
+        at = pl.ds(pl.multiple_of(own * L + i * step, step), step)
         total = acc[at, :] + sbi[at, :].astype(F32)
-        for dq in range(1, ng):
+        for dq in (1, 2):
             total = total + rdi[dq - 1, pl.ds(pl.multiple_of(i * step, step), step), :].astype(F32)
         return total.astype(BF16).astype(F32)
 
     def wait_reduced(rdi, k):
-        for dq in range(1, ng):
+        for dq in (1, 2):
             arrived(rdi.at[dq - 1], rsem.at[k, 0], rsem.at[k, 2 * dq + 1])
 
-    whole(2)
-    reduce_rows(hid, fmo, sbo1, sbi1, rdo1, rdi1, 0)
+    line_whole(2)
+
+    def before_partial():
+        send(3, 2, (0,), outer)
+        got_and_send(3, (2, 3), None, inner)
+
+    reduce_rows(hid, fmo, sbo1, sbi1, rdo1, rdi1, 0, seat, seat_fs, before_partial)
+    send(3, 2, (1, 2, 3), outer)
+    relay(3, when=inner)
+    got_and_send(4, (2, 3), inner, inner)
     wait_reduced(rdi1, 0)
 
     def resid_rows(i, _):
         at = pl.ds(pl.multiple_of(i * step, step), step)
         own = tok[pl.ds(pl.multiple_of(t * L + i * step, step), step), :].astype(F32)
-        value = own + reduced(sbi1, rdi1, i)
+        value = own + reduced(sbi1, rdi1, s, i)
         resid[at, :] = value
         scale = lax.rsqrt(jnp.mean(value * value, axis=-1, keepdims=True) + norm_floor)
         nm_all[pl.ds(pl.multiple_of(t * half + p * L + i * step, step), step), :] = (
@@ -396,15 +518,14 @@
         return 0
 
     lax.fori_loop(0, L // step, resid_rows, 0)
-    mine = nm_all.at[rows_at(t * half + p * L, L)]
-    for dq in range(1, ng):
-        push(mine, mine, nsem.at[0, dq], nsem.at[1, dq], (fs_of(dq, 0), t))
-    push(mine, mine, nsem.at[2, 0], nsem.at[3, 0], (f, sib))
-    relay(3)
-    for dq in range(1, ng):
-        block = nm_all.at[rows_at(t * half + chip(dq) * L, L)]
-        arrived(block, nsem.at[0, 0], nsem.at[1, dq])
-        push(block, block, nsem.at[2, dq], nsem.at[3, dq], (f, sib))
+    gather_start(*second)
+    relay(3, when=outer)
+    gather_relay(second, 2)
+    got_and_send(4, (2, 3), outer)
+    send(4, 2, when=outer)
+    relay(4, (0, 1), inner)
+    gather_relay(second, 1, 3)
+    relay(4, (2, 3), inner)
 
     whole(3)
 
@@ -421,18 +542,16 @@
         lax.fori_loop(0, hidden // 256, body, 0)
 
     up_half(t)
-    relay(4, (0, 1))
-    for dq in range(ng):
-        arrived(nm_all.at[rows_at(sib * half + chip(dq) * L, L)], nsem.at[0, 0], nsem.at[3, dq])
+    gather_finish(second, 0, 1, 2, 3)
     up_half(sib)
-    relay(4, (2, 3))
+    relay(4, when=outer)
     whole(4)
-    reduce_rows(act, fdn, sbo2, sbi2, rdo2, rdi2, 1)
+    reduce_rows(act, fdn, sbo2, sbi2, rdo2, rdi2, 1, chip, fs_of)
     wait_reduced(rdi2, 1)
 
     def finish_rows(i, _):
         at = pl.ds(pl.multiple_of(i * step, step), step)
-        value = (resid[at, :] + reduced(sbi2, rdi2, i)).astype(BF16)
+        value = (resid[at, :] + reduced(sbi2, rdi2, p, i)).astype(BF16)
         fin[0, at, :] = value
         out[pl.ds(pl.multiple_of(t * L + i * step, step), step), :] = value
         return 0
@@ -447,8 +566,8 @@
         return 0
 
     lax.fori_loop(0, L // step, copy_rows, 0)
-    for copy in sends:
-        copy.wait_send()
+    for copy, when in sends:
+        act_if(when, copy.wait_send)
 
 
 def fused_device(ng, nz, tokens, mix_gain, glu_value, glu_gate, conv_taps, chan_gain, mix_out, mlp_gain, up_weight, down_weight):
@@ -469,7 +588,7 @@
     scratch = [
         vm((fs * depth, chans), BF16), vm((fs * depth, chans), BF16), vm((chans, width), BF16),
         vm((fs * depth, hidden), BF16), vm((hidden, width), BF16),
-        vm((2 * half, width), BF16), vm((2 * half, width), BF16),
+        vm((2 * half, width), BF16),
         vm((L + 32, chans), F32), vm((2 * half, chans), F32), vm((2 * half, chans), BF16),
         vm((blocks, 8, L), F32), vm((blocks, blocks, 8, L), F32),
         vm((half, width), F32), vm((L, width), F32), vm((2 * half, width), BF16),

time: 252 us -> 208 us (0.83)
  Pallas kernels: 250 us -> 205 us
    pallas_call x1, Pallas kernels: 250 us -> 205 us  [fused_device(): pl.pallas_call(functools.partial(layer_kernel, ng), out_shape=jax.ShapeDt...]
where the time goes in v1:
time: 208 us; the launch traced here: 207 us
  Pallas kernels  205 us (99%)
  local copies, waits for them, and re-layouts  2.3 us (1%)
    pallas_call x1, Pallas kernels, fused_device(): pl.pallas_call(functools.partial(layer_kernel, ng), out_shape=jax.ShapeDt...  205 us

profile of v1, /device:TPU:0, one launch (start us, length us, event | category | flops | bytes accessed | tf_op | source)
XLA Modules:
  0.0 206.9 jit_solution(6381183581980655378)
XLA Ops:
  0.0 204.6 %shard_map.100 = bf16[256,2048]{1,0:T(8,128)(2,1)} custom-call(bf16[256,2048]{1,0:T(8,128)(2,1)} %tok.1, f32[1,2048]{1,0:T(1,128)} %bitcast.3, bf16[128,1024]{1,0:T(8,128)(2,1)} %gv.1, bf16[128,1024]{1,0:T(8,128)(2,1)} %gg.1, f32[31,1024]{1,0:T(8,128)} %taps.1, f32[1,1024]{1,0:T(1,128)} %bitcast.5, bf16[1024,128]{1,0:T(8,128)(2,1)} %mo.1, ...), custom_call_target="tpu_custom_call" | custom-call | tf_op jit(solution)/shard_map/pallas_call | solution.py:600
  204.6 2.3 %copy.12 = bf16[256,2048]{1,0:T(8,128)(2,1)} copy(bf16[256,2048]{1,0:T(8,128)(2,1)} %shard_map.100) | data formatting | bytes 2097152

commit v2 on v1

--- a/solution.py
+++ b/solution.py
@@ -117,6 +117,42 @@
 F32, BF16 = jnp.float32, jnp.bfloat16
 
 
+OUTER = (
+    ("P01", "P02", "P03", "P11", "P12", "P13", "O00", "O10",),
+    ("P21", "P22", "P23", "W0", "O01", "W1", "O11", "O20",),
+    ("P31", "Y30", "X33", "P41", "Y40", "X43", "W2", "O21", "D33", "P32",),
+    ("D43", "P42",),
+    ("G41",),
+    ("Z30", "G31", "Z31",),
+    (),
+    ("G32", "G33", "Z32", "Z33", "R30",),
+    ("R31", "R32", "R33",),
+    ("G42", "G43", "Z40", "Z41", "Z42", "Z43",),
+    (),
+    ("R40",),
+    ("R41",),
+    ("R42",),
+    ("R43",),
+)
+INNER = (
+    ("P01", "P02", "P03", "P11", "P12", "O10", "P13", "O00", "Q00", "Q10",),
+    ("P21", "P22", "P23", "W0", "O01", "Q01", "W1", "O11", "Q11", "O20", "Q20",),
+    ("P31", "Y30", "X33", "P41", "Y40", "X43", "N0", "N1", "M0", "M1", "W2", "F0", "O21", "F1", "Q21", "N2", "Z30",),
+    ("M2", "G31", "Z31",),
+    ("F2", "D33", "Z40", "P32", "G41", "Z41",),
+    (),
+    ("G32", "Z32", "G33", "Z33", "D43", "P42",),
+    ("R30", "R31", "G42", "Z42", "G43", "Z43",),
+    ("R32", "R33",),
+    ("R40", "R41",),
+    ("R42", "R43",),
+    (),
+    (),
+    (),
+    (),
+)
+
+
 def rows_at(start, size):
     return pl.ds(pl.multiple_of(start, 128), size)
 
@@ -125,11 +161,11 @@
     ng,
     tok, mixg, gv, gg, taps, chg, mo, mlpg, up, dn,
     out,
-    fgv, fgg, fmo, fup, fdn,
-    nrm, pad, cv, hid, st, st_all,
+    fgv, fgg, fmo, fup, fdn, stage_up, stage_dn,
+    nrm, pad, phase, cv, hid, st, st_all,
     acc, resid, nm_all, act, fin,
     sbo1, sbi1, rdo1, rdi1, sbo2, sbi2, rdo2, rdi2,
-    ws, wr, lsem, tsem, nsem, ssem, rsem, fsem,
+    ws, wr, lsem, tsem, nsem, ssem, rsem, dsem, fsem,
 ):
     f, t = lax.axis_index("fs"), lax.axis_index("tp")
     x, y = lax.rem(f, 2), lax.rem(lax.div(f, 2), 2)
@@ -142,7 +178,7 @@
     chans = fgv.shape[1]
     hidden = fup.shape[1]
     depth = gv.shape[0]
-    sends, sent = [], set()
+    sends = []
 
     def flip(coord, bit):
         return 1 - coord if bit else coord
@@ -172,24 +208,10 @@
             device_id=device, device_id_type=MESH,
         )
 
-    def act_if(when, act):
-        if when is None:
-            act()
-        else:
-            pl.when(when)(act)
-
-    def start(src, dst, s_sem, r_sem, device, when=None):
-        copy = remote(src, dst, s_sem, r_sem, device)
-        act_if(when, copy.start)
-        return copy
-
-    def push(src, dst, s_sem, r_sem, device, when=None):
-        sends.append((start(src, dst, s_sem, r_sem, device, when), when))
-
-    def once(key, copy):
-        if key not in sent:
-            sent.add(key)
-            sends.append((copy, None))
+    def push(*args):
+        copy = remote(*args)
+        copy.start()
+        sends.append(copy)
 
     def arrived(dst, s_sem, r_sem):
         remote(dst, dst, s_sem, r_sem, (f, sib)).wait_recv()
@@ -199,7 +221,6 @@
     peers += [(f, sib), (near, t), (fs_of(3, 0), t), (mate, t)]
     for peer in peers:
         pl.semaphore_signal(barrier, inc=1, device_id=peer, device_id_type=MESH)
-    pl.semaphore_wait(barrier, len(peers))
 
     weights = (
         (lambda q: gv.at[:, rows_at(q * chans, chans)], lambda g: fgv.at[rows_at(g * depth, depth), :]),
@@ -209,48 +230,68 @@
         (lambda q: dn.at[rows_at(q * hidden, hidden), :], lambda g: fdn.at[:, rows_at(g * depth, depth)]),
     )
 
-    def spread_in_plane(a, which=(1, 2, 3), when=None):
+    stage = (stage_up, stage_dn)
+
+    def parts(op):
+        kind, a, dq = op[0], int(op[1]), int((op + "0")[2])
         src, dst = weights[a]
         part, place = (seat, seat_fs) if a < 3 else (chip, fs_of)
-        for dq in which:
-            copy = start(src(part(dq)), dst(f), ws.at[a, dq], wr.at[a, dq], (place(dq, 0), t), when)
-            once((a, 0, dq), copy)
-
-    def send(a, do, which=(0, 1, 2, 3), when=None):
-        src, dst = weights[a]
-        for dq in which:
+
+        def mk(s_at, r_at, piece, to, own=None):
+            return remote(piece if own is None else own, piece, ws.at[a, s_at], wr.at[a, r_at], (to, t))
+
+        if kind == "P":
+            return [], [mk(dq, dq, dst(f), place(dq, 0), src(part(dq)))]
+        if kind == "X":
+            return [], [mk(0, 0, stage[a - 3], fs_of(1, 0), src(chip(3)))]
+        if kind == "D":
+            return [mk(0, 0, stage[a - 3], f)], [mk(3, 3, dst(fs_of(1, 0)), near, stage[a - 3])]
+        if kind == "W":
+            return [mk(0, i, dst(place(i, 0)), f) for i in (1, 2, 3)], []
+        if kind in "YGZ":
+            do = 2 if kind == "Z" else 1
             piece = dst(fs_of(dq, 0))
-            copy = start(
-                src(p) if dq == 0 else piece, piece,
-                ws.at[a, do * ng + dq], wr.at[a, do * ng + dq], (fs_of(0, do), t), when,
-            )
-            once((a, do, dq), copy)
-
-    def got(a, dq, when=None):
-        piece = weights[a][1]((seat_fs if a < 3 else fs_of)(dq, 0))
-        come = remote(piece, piece, ws.at[a, 0], wr.at[a, dq], (f, sib))
-        act_if(when, come.wait_recv)
-
-    def got_and_send(a, which, when=None, zh_when=None):
-        for dq in which:
-            got(a, dq, when)
-            send(a, 1, (dq,), when)
-            if zh_when is not None:
-                send(a, 2, (dq,), zh_when)
-
-    def relay(a, which=(0, 1, 2, 3), when=None):
-        dst = weights[a][1]
-        for dq in which:
+            come = [mk(0, dq, piece, f)] if kind == "G" else []
+            k = do * ng + dq
+            return come, [mk(k, k, piece, fs_of(0, do), src(p) if dq == 0 else None)]
+        if kind == "R":
             piece = dst(fs_of(dq, 2))
-            come = remote(piece, piece, ws.at[a, 0], wr.at[a, 2 * ng + dq], (f, sib))
-            copy = remote(piece, piece, ws.at[a, 3 * ng + dq], wr.at[a, 3 * ng + dq], (fs_of(0, 1), t))
-
-            def pass_on():
-                come.wait_recv()
+            k = 3 * ng + dq
+            return [mk(0, 2 * ng + dq, piece, f)], [mk(k, k, piece, fs_of(0, 1))]
+        plane = planes[a]
+        if kind in "OQ":
+            k, to = (4, near) if kind == "O" else (8, mate)
+            own = src(part(0))
+            return [], [mk(k + i, k + i, dst(place(i, 0)), to, None if i else own) for i in ((1, 2, 3) if dq else (0,))]
+        if kind == "N":
+            return [mk(0, 4 + i, dst(line_fs(z_near, i)), f) for i in range(4)], [mk(12, 12, plane(z_near), mate)]
+        if kind == "M":
+            return [mk(0, 8 + i, dst(line_fs(z_mate, i)), f) for i in range(4)], [mk(13, 13, plane(z_mate), near)]
+        return [mk(0, 12, plane(z_far), f)], [mk(14, 14, plane(z_far), near)]
+
+    def run(ops):
+        for op in ops:
+            come, go = parts(op)
+            for copy in come:
+                copy.wait_recv()
+            if op[0] == "W":
+                local(int(op[1])).wait()
+            for copy in go:
                 copy.start()
 
-            act_if(when, pass_on)
-            once((a, 3, dq), copy)
+    def drain(plan):
+        for ops in plan:
+            for op in ops:
+                for copy in parts(op)[1]:
+                    copy.wait_send()
+
+    def gap(i):
+        if OUTER[i] == INNER[i]:
+            run(OUTER[i])
+            return
+        for plan, when in ((OUTER, outer), (INNER, inner)):
+            if plan[i]:
+                pl.when(when)(functools.partial(run, plan[i]))
 
     def whole(a):
         dst = weights[a][1]
@@ -269,34 +310,14 @@
         lambda g: fmo.at[:, rows_at(g * ng * depth, ng * depth)],
     )
 
-    def line(a, g, s_at, r_at, to, when=None):
-        block = planes[a](g)
-        push(block, block, ws.at[a, s_at], wr.at[a, r_at], (to, t), when)
-
-    def line_got(a, g, r_at, when):
-        come = remote(planes[a](g), planes[a](g), ws.at[a, 0], wr.at[a, r_at], (f, sib))
-        act_if(when, come.wait_recv)
-
-    def line_own(a, when=None):
-        line(a, z, 4, 4, near, when)
-        if when is not outer:
-            line(a, z, 7, 5, mate, inner)
-
-    def line_near(a):
-        line_got(a, z_near, 4, inner)
-        line(a, z_near, 8, 6, mate, inner)
-
-    def line_mate(a):
-        line_got(a, z_mate, 5, inner)
-        line(a, z_mate, 5, 5, near, inner)
-
-    def line_far(a):
-        line_got(a, z_far, 6, inner)
-        line(a, z_far, 6, 6, near, inner)
+    def line_fs(g, i):
+        return g * ng + seat(i)
 
     def line_whole(a):
-        for g, r_at in ((z_near, 4), (z_mate, 5), (z_far, 6)):
-            line_got(a, g, r_at, outer)
+        for i in range(ng):
+            arrived(weights[a][1](line_fs(z_near, i)), ws.at[a, 0], wr.at[a, 4 + i])
+        for g, r_at in ((z_mate, 13), (z_far, 14)):
+            arrived(planes[a](g), ws.at[a, 0], wr.at[a, r_at])
 
     first = (nrm, tsem, seat, seat_fs)
     second = (nm_all, nsem, chip, fs_of)
@@ -337,77 +358,75 @@
     def from_ref(ref, base):
         return lambda i: ref[pl.ds(pl.multiple_of(base + i, step), step), :]
 
-    for a in (0, 1):
-        spread_in_plane(a)
+    norm_rows(from_ref(tok, t * L), mixg, nrm, t * half + s * L)
+    pl.semaphore_wait(barrier, len(peers))
+    gap(0)
     for a in range(5):
         local(a).start()
-    norm_rows(from_ref(tok, t * L), mixg, nrm, t * half + s * L)
     gather_start(*first)
-    spread_in_plane(2)
-
-    def plane_ready(a):
-        for dq in (1, 2, 3):
-            got(a, dq)
-        local(a).wait()
-
-    for a in (0, 1):
-        plane_ready(a)
-        line_own(a)
+    gap(1)
     gather_relay(first, 2, 1)
-    for a in (3, 4):
-        spread_in_plane(a, (1,))
-        send(a, 1, (0,))
-    for step_of in (line_near, line_mate):
-        for a in (0, 1):
-            step_of(a)
-    plane_ready(2)
-    line_own(2, outer)
-    for a in (0, 1):
-        line_far(a)
-    line_own(2, inner)
-    line_near(2)
-    send(3, 2, (0,), inner)
-    spread_in_plane(3, (3, 2), outer)
+    gap(2)
     gather_finish(first, 0, 1)
-    for a in (0, 1):
-        line_whole(a)
+
+    @pl.when(outer)
+    def _():
+        line_whole(0)
+        line_whole(1)
+
     pad[...] = jnp.zeros_like(pad)
     st[...] = jnp.zeros_like(st)
     taps_n = taps.shape[0]
     reach = taps_n // 2
     lead = (reach + 7) // 8 * 8
+    reach_lead = lead - reach
     own_cols = s * chans
     eye = lax.broadcasted_iota(jnp.int32, (L, L), 0) == lax.broadcasted_iota(jnp.int32, (L, L), 1)
 
-    def conv_block(i, _):
-        b = lax.rem(i, 2) * ng + lax.rem(y + lax.div(i, 4), 2) * 2 + lax.rem(x + lax.div(i, 2), 2)
-        rows = rows_at(b * L, L)
-        left = nrm[rows, :]
-        values = jnp.dot(left, fgv[...], preferred_element_type=F32)
-        gating = jnp.dot(left, fgg[...], preferred_element_type=F32)
-        glu = (values * jax.nn.sigmoid(gating)).astype(BF16).astype(F32)
-        pad[pl.ds(lead, L), :] = glu
-        sums = jnp.zeros((L, 1), F32)
-        squares = jnp.zeros((L, 1), F32)
-        for c in range(chans // 128):
-            total = jnp.zeros((L, 128), F32)
-            for j in range(taps_n):
-                tap = taps[pl.ds(j, 1), rows_at(own_cols + c * 128, 128)]
-                total = total + pad[pl.ds(lead - reach + j, L), pl.ds(c * 128, 128)] * tap
-            cv[rows, pl.ds(c * 128, 128)] = total
-            sums = sums + jnp.sum(total, axis=1, keepdims=True)
-            squares = squares + jnp.sum(total * total, axis=1, keepdims=True)
-        st[b, pl.ds(0, 1), :] = jnp.sum(jnp.where(eye, sums, 0.0), axis=0, keepdims=True)
-        st[b, pl.ds(1, 1), :] = jnp.sum(jnp.where(eye, squares, 0.0), axis=0, keepdims=True)
-        return 0
-
-    lax.fori_loop(0, ng, conv_block, 0)
+    def conv_half(pair_base):
+        def glu_rows(u, _):
+            rows = rows_at(u * half + pair_base * L, 2 * L)
+            left = nrm[rows, :]
+            values = jnp.dot(left, fgv[...], preferred_element_type=F32)
+            gating = jnp.dot(left, fgg[...], preferred_element_type=F32)
+            cv[rows, :] = (values * jax.nn.sigmoid(gating)).astype(BF16).astype(F32)
+            return 0
+
+        def conv_block(i, _):
+            b = lax.rem(i, 2) * ng + pair_base + lax.div(i, 2)
+            rows = rows_at(b * L, L)
+            sums = jnp.zeros((L, 1), F32)
+            squares = jnp.zeros((L, 1), F32)
+            for c in range(chans // 128):
+                at = pl.ds(c * 128, 128)
+                pad[pl.ds(lead, L), :] = cv[rows, at]
+                window = pad[...]
+                for r in range(8):
+                    partial = jnp.zeros((L + 8, 128), F32)
+                    for m in range(lead // 4):
+                        j = 8 * m + r - reach_lead
+                        if 0 <= j < taps_n:
+                            tap = taps[pl.ds(j, 1), rows_at(own_cols + c * 128, 128)]
+                            partial = partial + window[8 * m : 8 * m + L + 8] * tap
+                    phase[r] = partial
+                total = phase[0, pl.ds(0, L), :]
+                for r in range(1, 8):
+                    total = total + phase[r, pl.ds(r, L), :]
+                cv[rows, at] = total
+                sums = sums + jnp.sum(total, axis=1, keepdims=True)
+                squares = squares + jnp.sum(total * total, axis=1, keepdims=True)
+            st[b, pl.ds(0, 1), :] = jnp.sum(jnp.where(eye, sums, 0.0), axis=0, keepdims=True)
+            st[b, pl.ds(1, 1), :] = jnp.sum(jnp.where(eye, squares, 0.0), axis=0, keepdims=True)
+            return 0
+
+        lax.fori_loop(0, 2, glu_rows, 0)
+        lax.fori_loop(0, ng, conv_block, 0)
+
+    conv_half(y * 2)
     gather_relay(first, 3)
-    line_mate(2)
-    got_and_send(3, (1,), None, inner)
-    spread_in_plane(4, (3, 2), outer)
+    gap(3)
     gather_finish(first, 2, 3)
-    lax.fori_loop(ng, 2 * ng, conv_block, 0)
+    conv_half((1 - y) * 2)
 
     slots = [(dq, du) for dq in range(ng) for du in range(2) if (dq, du) != (0, 0)]
     for dq, du in slots:
@@ -416,11 +435,7 @@
             ssem.at[0, dq * 2 + du], ssem.at[1, dq * 2 + du],
             (seat_fs(dq), t if du == 0 else sib),
         )
-    line_far(2)
-    spread_in_plane(3, (3, 2), inner)
-    spread_in_plane(4, (3, 2), inner)
-    send(4, 2, (0,), inner)
-    got_and_send(4, (1,), None, inner)
+    gap(4)
     for dq, du in slots:
         arrived(st_all.at[dq * 2 + du], ssem.at[0, 0], ssem.at[1, dq * 2 + du])
 
@@ -442,74 +457,79 @@
     lax.fori_loop(0, 2 * ng, hidden_block, 0)
 
     cols = 512
-
-    def reduce_rows(left, right, sbo, sbi, rdo, rdi, k, part, place, between=lambda: None):
-        def theirs(n, _):
-            at = rows_at(n * cols, cols)
-            sbo[:, at] = jnp.dot(
-                left[rows_at(sib * half, half), :], right[:, at], preferred_element_type=F32
+    span = 32
+    chunks = [pl.ds(n * cols, cols) for n in range(width // cols)]
+
+    def over_rows(body):
+        def go(i, _):
+            body(pl.multiple_of(i * span, span))
+            return 0
+
+        lax.fori_loop(0, L // span, go, 0)
+
+    def mix_partial(n, dq):
+        at, base = chunks[n], seat(dq) * L
+
+        def add(i):
+            row = pl.ds(pl.multiple_of(base + i, span), span)
+            total = acc[row, at] + sbi1[row, at].astype(F32)
+            if dq == 2:
+                total = total + rdi1[2, pl.ds(i, span), at].astype(F32)
+            rdo1[row, at] = total.astype(BF16)
+
+        over_rows(add)
+        push(
+            rdo1.at[rows_at(base, L), at], rdi1.at[dq - 1, :, at],
+            rsem.at[0, dq, n], rsem.at[1, dq, n], (seat_fs(2 if dq == 2 else 1), t),
+        )
+
+    def reduce_mixed():
+        for n, at in enumerate(chunks):
+            sbo1[:, at] = jnp.dot(
+                hid[rows_at(sib * half, half), :], fmo[:, at], preferred_element_type=F32
             ).astype(BF16)
-            return 0
-
-        lax.fori_loop(0, width // cols, theirs, 0)
-        push(sbo, sbi, rsem.at[k, 0], rsem.at[k, 1], (f, sib))
+            push(sbo1.at[:, at], sbi1.at[:, at], rsem.at[0, 0, n], rsem.at[1, 0, n], (f, sib))
 
         def mine(n, _):
             at = rows_at(n * cols, cols)
             acc[:, at] = jnp.dot(
-                left[rows_at(t * half, half), :], right[:, at], preferred_element_type=F32
+                hid[rows_at(t * half, half), :], fmo[:, at], preferred_element_type=F32
             )
             return 0
 
         lax.fori_loop(0, width // cols, mine, 0)
-        arrived(sbi, rsem.at[k, 0], rsem.at[k, 1])
-        for dq in (3, 1, 2):
-            base = part(dq) * L
-            if dq == 2:
-                between()
-                arrived(rdi.at[2], rsem.at[k, 0], rsem.at[k, 7])
-
-            def add(i, _):
-                at = pl.ds(pl.multiple_of(base + i * step, step), step)
-                total = acc[at, :] + sbi[at, :].astype(F32)
-                if dq == 2:
-                    total = total + rdi[2, pl.ds(pl.multiple_of(i * step, step), step), :].astype(F32)
-                rdo[at, :] = total.astype(BF16)
-                return 0
-
-            lax.fori_loop(0, L // step, add, 0)
-            push(
-                rdo.at[rows_at(base, L)], rdi.at[dq - 1],
-                rsem.at[k, 2 * dq], rsem.at[k, 2 * dq + 1], (place(2 if dq == 2 else 1, 0), t),
-            )
-
-    def reduced(sbi, rdi, own, i):
-        at = pl.ds(pl.multiple_of(own * L + i * step, step), step)
-        total = acc[at, :] + sbi[at, :].astype(F32)
+        for dq in (3, 1):
+            for n, at in enumerate(chunks):
+                if dq == 3:
+                    arrived(sbi1.at[:, at], rsem.at[0, 0, 0], rsem.at[1, 0, n])
+                mix_partial(n, dq)
+        gap(6)
+        for n, at in enumerate(chunks):
+            arrived(rdi1.at[2, :, at], rsem.at[0, 0, 0], rsem.at[1, 3, n])
+            mix_partial(n, 2)
+
+    def reduced(i):
+        at = pl.ds(pl.multiple_of(s * L + i * step, step), step)
+        total = acc[at, :] + sbi1[at, :].astype(F32)
         for dq in (1, 2):
-            total = total + rdi[dq - 1, pl.ds(pl.multiple_of(i * step, step), step), :].astype(F32)
+            total = total + rdi1[dq - 1, pl.ds(pl.multiple_of(i * step, step), step), :].astype(F32)
         return total.astype(BF16).astype(F32)
 
-    def wait_reduced(rdi, k):
-        for dq in (1, 2):
-            arrived(rdi.at[dq - 1], rsem.at[k, 0], rsem.at[k, 2 * dq + 1])
-
-    line_whole(2)
-
-    def before_partial():
-        send(3, 2, (0,), outer)
-        got_and_send(3, (2, 3), None, inner)
-
-    reduce_rows(hid, fmo, sbo1, sbi1, rdo1, rdi1, 0, seat, seat_fs, before_partial)
-    send(3, 2, (1, 2, 3), outer)
-    relay(3, when=inner)
-    got_and_send(4, (2, 3), inner, inner)
-    wait_reduced(rdi1, 0)
+    @pl.when(outer)
+    def _():
+        line_whole(2)
+
+    gap(5)
+    reduce_mixed()
+    gap(7)
+    for dq in (1, 2):
+        for n, at in enumerate(chunks):
+            arrived(rdi1.at[dq - 1, :, at], rsem.at[0, 0, 0], rsem.at[1, dq, n])
 
     def resid_rows(i, _):
         at = pl.ds(pl.multiple_of(i * step, step), step)
         own = tok[pl.ds(pl.multiple_of(t * L + i * step, step), step), :].astype(F32)
-        value = own + reduced(sbi1, rdi1, s, i)
+        value = own + reduced(i)
         resid[at, :] = value
         scale = lax.rsqrt(jnp.mean(value * value, axis=-1, keepdims=True) + norm_floor)
         nm_all[pl.ds(pl.multiple_of(t * half + p * L + i * step, step), step), :] = (
@@ -519,14 +539,11 @@
 
     lax.fori_loop(0, L // step, resid_rows, 0)
     gather_start(*second)
-    relay(3, when=outer)
+    gap(8)
     gather_relay(second, 2)
-    got_and_send(4, (2, 3), outer)
-    send(4, 2, when=outer)
-    relay(4, (0, 1), inner)
+    gap(9)
     gather_relay(second, 1, 3)
-    relay(4, (2, 3), inner)
-
+    gap(10)
     whole(3)
 
     def up_half(u):
@@ -541,33 +558,116 @@
 
         lax.fori_loop(0, hidden // 256, body, 0)
 
+    gap(11)
     up_half(t)
+    gap(12)
     gather_finish(second, 0, 1, 2, 3)
     up_half(sib)
-    relay(4, when=outer)
-    whole(4)
-    reduce_rows(act, fdn, sbo2, sbi2, rdo2, rdi2, 1, chip, fs_of)
-    wait_reduced(rdi2, 1)
-
-    def finish_rows(i, _):
-        at = pl.ds(pl.multiple_of(i * step, step), step)
-        value = (resid[at, :] + reduced(sbi2, rdi2, p, i)).astype(BF16)
-        fin[0, at, :] = value
-        out[pl.ds(pl.multiple_of(t * L + i * step, step), step), :] = value
-        return 0
-
-    lax.fori_loop(0, L // step, finish_rows, 0)
-    push(fin.at[0], fin.at[1], fsem.at[0], fsem.at[1], (f, sib))
-    arrived(fin.at[1], fsem.at[0], fsem.at[1])
-
-    def copy_rows(i, _):
-        at = pl.ds(pl.multiple_of(i * step, step), step)
-        out[pl.ds(pl.multiple_of(sib * L + i * step, step), step), :] = fin[1, at, :]
-        return 0
-
-    lax.fori_loop(0, L // step, copy_rows, 0)
-    for copy, when in sends:
-        act_if(when, copy.wait_send)
+
+    pair = 2 * depth
+    def pair_at(g, j):
+        return rows_at((flip(zh, g // 2) * 8 + j * 4 + flip(y, g % 2) * 2) * depth, pair)
+
+    def down_group(g):
+        def theirs(j, _):
+            at = pair_at(g, j)
+            sbo2[:, at] = jnp.dot(
+                act[rows_at(sib * half, half), :], fdn[:, at], preferred_element_type=F32
+            ).astype(BF16)
+            return 0
+
+        def mine(j, _):
+            at = pair_at(g, j)
+            acc[:, at] = jnp.dot(
+                act[rows_at(t * half, half), :], fdn[:, at], preferred_element_type=F32
+            )
+            return 0
+
+        lax.fori_loop(0, 2, theirs, 0)
+        for j in range(2):
+            at = pair_at(g, j)
+            push(sbo2.at[:, at], sbi2.at[:, at], dsem.at[0, g * 2 + j, 0], dsem.at[1, g * 2 + j, 0], (f, sib))
+        lax.fori_loop(0, 2, mine, 0)
+        for j in range(2):
+            arrived(sbi2.at[:, pair_at(g, j)], dsem.at[0, 0, 0], dsem.at[1, g * 2 + j, 0])
+        for dq in (3, 1):
+            for j in range(2):
+                pass_partial(g, j, dq)
+
+    def pass_partial(g, j, dq):
+        at, base = pair_at(g, j), chip(dq) * L
+
+        def add(i):
+            row = pl.ds(pl.multiple_of(base + i, span), span)
+            total = acc[row, at] + sbi2[row, at].astype(F32)
+            if dq == 2:
+                total = total + rdi2[2, pl.ds(i, span), at].astype(F32)
+            rdo2[row, at] = total.astype(BF16)
+
+        over_rows(add)
+        push(
+            rdo2.at[rows_at(base, L), at], rdi2.at[dq - 1, :, at],
+            dsem.at[0, g * 2 + j, dq], dsem.at[1, g * 2 + j, dq], (fs_of(2 if dq == 2 else 1, 0), t),
+        )
+
+    def down_near(g):
+        for j in range(2):
+            arrived(rdi2.at[2, :, pair_at(g, j)], dsem.at[0, 0, 0], dsem.at[1, g * 2 + j, 3])
+            pass_partial(g, j, 2)
+
+    def down_final(g):
+        for j in range(2):
+            at = pair_at(g, j)
+            for dq in (1, 2):
+                arrived(rdi2.at[dq - 1, :, at], dsem.at[0, 0, 0], dsem.at[1, g * 2 + j, dq])
+
+            def finish(i):
+                row = pl.ds(pl.multiple_of(p * L + i, span), span)
+                here = pl.ds(i, span)
+                total = acc[row, at] + sbi2[row, at].astype(F32)
+                total = total + rdi2[0, here, at].astype(F32) + rdi2[1, here, at].astype(F32)
+                value = (resid[here, at] + total.astype(BF16).astype(F32)).astype(BF16)
+                fin[0, here, at] = value
+                out[pl.ds(pl.multiple_of(t * L + i, span), span), at] = value
+
+            over_rows(finish)
+            push(fin.at[0, :, at], fin.at[1, :, at], fsem.at[0, g * 2 + j], fsem.at[1, g * 2 + j], (f, sib))
+
+    def down_copy(g):
+        for j in range(2):
+            at = pair_at(g, j)
+            arrived(fin.at[1, :, at], fsem.at[0, 0], fsem.at[1, g * 2 + j])
+            out[rows_at(sib * L, L), at] = fin[1, :, at]
+
+    def down_wait(do):
+        for dq in range(ng):
+            arrived(weights[4][1](fs_of(dq, do)), ws.at[4, 0], wr.at[4, do * ng + dq])
+
+    local(4).wait()
+    gap(13)
+    down_group(0)
+    gap(14)
+    down_wait(1)
+    down_group(1)
+    down_near(0)
+    down_group(2)
+    down_near(1)
+    down_final(0)
+    down_wait(3)
+    down_group(3)
+    down_near(2)
+    down_final(1)
+    down_copy(0)
+    down_near(3)
+    down_final(2)
+    down_copy(1)
+    down_final(3)
+    down_copy(2)
+    down_copy(3)
+    for copy in sends:
+        copy.wait_send()
+    for plan, when in ((OUTER, outer), (INNER, inner)):
+        pl.when(when)(functools.partial(drain, plan))
 
 
 def fused_device(ng, nz, tokens, mix_gain, glu_value, glu_gate, conv_taps, chan_gain, mix_out, mlp_gain, up_weight, down_weight):
@@ -588,14 +688,15 @@
     scratch = [
         vm((fs * depth, chans), BF16), vm((fs * depth, chans), BF16), vm((chans, width), BF16),
         vm((fs * depth, hidden), BF16), vm((hidden, width), BF16),
+        vm((depth, hidden), BF16), vm((hidden, depth), BF16),
         vm((2 * half, width), BF16),
-        vm((L + 32, chans), F32), vm((2 * half, chans), F32), vm((2 * half, chans), BF16),
+        vm((L + 32, 128), F32), vm((8, L + 8, 128), F32), vm((2 * half, chans), F32), vm((2 * half, chans), BF16),
         vm((blocks, 8, L), F32), vm((blocks, blocks, 8, L), F32),
         vm((half, width), F32), vm((L, width), F32), vm((2 * half, width), BF16),
         vm((2 * half, hidden), BF16), vm((2, L, width), BF16),
         *reduce_bufs, *reduce_bufs,
         dma((5, fs)), dma((5, fs)), dma((5,)), dma((4, ng)), dma((4, ng)),
-        dma((2, blocks)), dma((2, 2 * ng)), dma((2,)),
+        dma((2, blocks)), dma((2, ng, 4)), dma((2, 2 * ng, 4)), dma((2, 2 * ng)),
     ]
     return pl.pallas_call(
         functools.partial(layer_kernel, ng),

time: 208 us -> 178 us (0.86)
  Pallas kernels: 205 us -> 174 us
    pallas_call x1, Pallas kernels: 205 us -> 174 us  [fused_device(): pl.pallas_call(functools.partial(layer_kernel, ng), out_shape=jax.ShapeDt...]
where the time goes in v2:
time: 178 us; the launch traced here: 177 us
  Pallas kernels  174 us (98%)
  local copies, waits for them, and re-layouts  2.3 us (1%)
    pallas_call x1, Pallas kernels, fused_device(): pl.pallas_call(functools.partial(layer_kernel, ng), out_shape=jax.ShapeDt...  174 us

profile of v2, /device:TPU:0, one launch (start us, length us, event | category | flops | bytes accessed | tf_op | source)
XLA Modules:
  0.0 176.7 jit_solution(6920691646549884216)
XLA Ops:
  0.0 174.4 %shard_map.100 = bf16[256,2048]{1,0:T(8,128)(2,1)} custom-call(bf16[256,2048]{1,0:T(8,128)(2,1)} %tok.1, f32[1,2048]{1,0:T(1,128)} %bitcast.3, bf16[128,1024]{1,0:T(8,128)(2,1)} %gv.1, bf16[128,1024]{1,0:T(8,128)(2,1)} %gg.1, f32[31,1024]{1,0:T(8,128)} %taps.1, f32[1,1024]{1,0:T(1,128)} %bitcast.5, bf16[1024,128]{1,0:T(8,128)(2,1)} %mo.1, ...), custom_call_target="tpu_custom_call" | custom-call | tf_op jit(solution)/shard_map/pallas_call | solution.py:701
  174.4 2.3 %copy.12 = bf16[256,2048]{1,0:T(8,128)(2,1)} copy(bf16[256,2048]{1,0:T(8,128)(2,1)} %shard_map.100) | data formatting | bytes 2097152

commit v3 on v2

--- a/solution.py
+++ b/solution.py
@@ -118,14 +118,14 @@
 
 
 OUTER = (
-    ("P01", "P02", "P03", "P11", "P12", "P13", "O00", "O10",),
+    ("P01", "P02", "P03", "P11", "P12", "P13", "O00", "O10", "P32",),
     ("P21", "P22", "P23", "W0", "O01", "W1", "O11", "O20",),
-    ("P31", "Y30", "X33", "P41", "Y40", "X43", "W2", "O21", "D33", "P32",),
-    ("D43", "P42",),
-    ("G41",),
-    ("Z30", "G31", "Z31",),
-    (),
-    ("G32", "G33", "Z32", "Z33", "R30",),
+    ("P31", "Y30", "X33", "P41", "Y40", "X43", "W2", "O21", "D33", "G31",),
+    ("D43", "P42", "G41",),
+    ("G32",),
+    ("Z30", "Z31",),
+    ("G33", "Z32", "Z33",),
+    ("R30",),
     ("R31", "R32", "R33",),
     ("G42", "G43", "Z40", "Z41", "Z42", "Z43",),
     (),
@@ -135,14 +135,14 @@
     ("R43",),
 )
 INNER = (
-    ("P01", "P02", "P03", "P11", "P12", "O10", "P13", "O00", "Q00", "Q10",),
+    ("P01", "P02", "P03", "P11", "P12", "O10", "P13", "O00", "Q00", "Q10", "P32",),
     ("P21", "P22", "P23", "W0", "O01", "Q01", "W1", "O11", "Q11", "O20", "Q20",),
     ("P31", "Y30", "X33", "P41", "Y40", "X43", "N0", "N1", "M0", "M1", "W2", "F0", "O21", "F1", "Q21", "N2", "Z30",),
-    ("M2", "G31", "Z31",),
-    ("F2", "D33", "Z40", "P32", "G41", "Z41",),
+    ("M2", "G31", "Z31", "D33",),
+    ("F2", "Z40", "G41", "Z41", "G32", "Z32",),
     (),
-    ("G32", "Z32", "G33", "Z33", "D43", "P42",),
-    ("R30", "R31", "G42", "Z42", "G43", "Z43",),
+    ("G33", "Z33", "D43",),
+    ("R30", "R31", "G42", "P42", "Z42", "G43", "Z43",),
     ("R32", "R33",),
     ("R40", "R41",),
     ("R42", "R43",),
@@ -159,13 +159,13 @@
 
 def layer_kernel(
     ng,
-    tok, mixg, gv, gg, taps, chg, mo, mlpg, up, dn,
+    tok, mixg, gv_in, gg_in, taps, chg, mo_in, mlpg, up_in, dn_in,
     out,
-    fgv, fgg, fmo, fup, fdn, stage_up, stage_dn,
+    gv, gg, mo, up, dn, fgv, fgg, fmo, fup, fdn, stage_up, stage_dn,
     nrm, pad, phase, cv, hid, st, st_all,
     acc, resid, nm_all, act, fin,
     sbo1, sbi1, rdo1, rdi1, sbo2, sbi2, rdo2, rdi2,
-    ws, wr, lsem, tsem, nsem, ssem, rsem, dsem, fsem,
+    hsem, ws, wr, lsem, tsem, nsem, ssem, rsem, dsem, fsem,
 ):
     f, t = lax.axis_index("fs"), lax.axis_index("tp")
     x, y = lax.rem(f, 2), lax.rem(lax.div(f, 2), 2)
@@ -216,6 +216,12 @@
     def arrived(dst, s_sem, r_sem):
         remote(dst, dst, s_sem, r_sem, (f, sib)).wait_recv()
 
+    loads = [
+        pltpu.make_async_copy(src, dst, hsem.at[i])
+        for i, (src, dst) in enumerate(((gv_in, gv), (gg_in, gg), (mo_in, mo), (up_in, up), (dn_in, dn)))
+    ]
+    for load in loads:
+        load.start()
     barrier = pltpu.get_barrier_semaphore()
     peers = [(seat_fs(dq), u) for dq in range(1, ng) for u in (t, sib)]
     peers += [(f, sib), (near, t), (fs_of(3, 0), t), (mate, t)]
@@ -360,6 +366,8 @@
 
     norm_rows(from_ref(tok, t * L), mixg, nrm, t * half + s * L)
     pl.semaphore_wait(barrier, len(peers))
+    for load in loads:
+        load.wait()
     gap(0)
     for a in range(5):
         local(a).start()
@@ -685,7 +693,9 @@
         vm((half, width), BF16), vm((half, width), BF16), vm((half, width), BF16),
         vm((ng - 1, L, width), BF16),
     ]
+    held = (2, 3, 6, 8, 9)
     scratch = [
+        *(vm(w.shape, BF16) for w in (glu_value, glu_gate, mix_out, up_weight, down_weight)),
         vm((fs * depth, chans), BF16), vm((fs * depth, chans), BF16), vm((chans, width), BF16),
         vm((fs * depth, hidden), BF16), vm((hidden, width), BF16),
         vm((depth, hidden), BF16), vm((hidden, depth), BF16),
@@ -695,13 +705,13 @@
         vm((half, width), F32), vm((L, width), F32), vm((2 * half, width), BF16),
         vm((2 * half, hidden), BF16), vm((2, L, width), BF16),
         *reduce_bufs, *reduce_bufs,
-        dma((5, fs)), dma((5, fs)), dma((5,)), dma((4, ng)), dma((4, ng)),
+        dma((5,)), dma((5, fs)), dma((5, fs)), dma((5,)), dma((4, ng)), dma((4, ng)),
         dma((2, blocks)), dma((2, ng, 4)), dma((2, 2 * ng, 4)), dma((2, 2 * ng)),
     ]
     return pl.pallas_call(
         functools.partial(layer_kernel, ng),
         out_shape=jax.ShapeDtypeStruct((rows, width), BF16),
-        in_specs=[pl.BlockSpec(memory_space=vm)] * 10,
+        in_specs=[pl.BlockSpec(memory_space=pl.ANY if i in held else vm) for i in range(10)],
         out_specs=pl.BlockSpec(memory_space=vm),
         scratch_shapes=scratch,
         compiler_params=pltpu.CompilerParams(

time: 178 us -> 172 us (0.966)
  Pallas kernels: 174 us -> 170 us
    pallas_call x1, Pallas kernels: 174 us -> 170 us  [fused_device(): pl.pallas_call(functools.partial(layer_kernel, ng), out_shape=jax.ShapeDt...]
where the time goes in v3:
time: 172 us
  Pallas kernels  170 us (99%)
  local copies, waits for them, and re-layouts  2.3 us (1%)
    pallas_call x1, Pallas kernels, fused_device(): pl.pallas_call(functools.partial(layer_kernel, ng), out_shape=jax.ShapeDt...  170 us

profile of v3, /device:TPU:0, one launch (start us, length us, event | category | flops | bytes accessed | tf_op | source)
XLA Modules:
  0.0 171.9 jit_solution(7224601399740532026)
XLA Ops:
  0.0 169.6 %shard_map.100 = bf16[256,2048]{1,0:T(8,128)(2,1)} custom-call(bf16[256,2048]{1,0:T(8,128)(2,1)} %tok.1, f32[1,2048]{1,0:T(1,128)} %bitcast.3, bf16[128,1024]{1,0:T(8,128)(2,1)} %gv_in.1, bf16[128,1024]{1,0:T(8,128)(2,1)} %gg_in.1, f32[31,1024]{1,0:T(8,128)} %taps.1, f32[1,1024]{1,0:T(1,128)} %bitcast.5, bf16[1024,128]{1,0:T(8,128)(2,1)} %mo_in.1, ...), custom_call_target="tpu_custom_call" | custom-call | tf_op jit(solution)/shard_map/pallas_call | solution.py:711
  169.6 2.3 %copy.12 = bf16[256,2048]{1,0:T(8,128)(2,1)} copy(bf16[256,2048]{1,0:T(8,128)(2,1)} %shard_map.100) | data formatting | bytes 2097152

commit v4 on v3

--- a/solution.py
+++ b/solution.py
@@ -121,8 +121,8 @@
     ("P01", "P02", "P03", "P11", "P12", "P13", "O00", "O10", "P32",),
     ("P21", "P22", "P23", "W0", "O01", "W1", "O11", "O20",),
     ("P31", "Y30", "X33", "P41", "Y40", "X43", "W2", "O21", "D33", "G31",),
-    ("D43", "P42", "G41",),
-    ("G32",),
+    ("G32", "D43", "P42", "G41",),
+    (),
     ("Z30", "Z31",),
     ("G33", "Z32", "Z33",),
     ("R30",),

time: 172 us -> 172 us (level)
  no operation moved by 1% of the time
where the time goes in v4:
time: 172 us
  Pallas kernels  169 us (98%)
  local copies, waits for them, and re-layouts  2.3 us (1%)
    pallas_call x1, Pallas kernels, fused_device(): pl.pallas_call(functools.partial(layer_kernel, ng), out_shape=jax.ShapeDt...  169 us

profile of v4, /device:TPU:0, one launch (start us, length us, event | category | flops | bytes accessed | tf_op | source)
XLA Modules:
  0.0 171.8 jit_solution(3611134201261787455)
XLA Ops:
  0.0 169.5 %shard_map.100 = bf16[256,2048]{1,0:T(8,128)(2,1)} custom-call(bf16[256,2048]{1,0:T(8,128)(2,1)} %tok.1, f32[1,2048]{1,0:T(1,128)} %bitcast.3, bf16[128,1024]{1,0:T(8,128)(2,1)} %gv_in.1, bf16[128,1024]{1,0:T(8,128)(2,1)} %gg_in.1, f32[31,1024]{1,0:T(8,128)} %taps.1, f32[1,1024]{1,0:T(1,128)} %bitcast.5, bf16[1024,128]{1,0:T(8,128)(2,1)} %mo_in.1, ...), custom_call_target="tpu_custom_call" | custom-call | tf_op jit(solution)/shard_map/pallas_call | solution.py:711
  169.5 2.3 %copy.12 = bf16[256,2048]{1,0:T(8,128)(2,1)} copy(bf16[256,2048]{1,0:T(8,128)(2,1)} %shard_map.100) | data formatting | bytes 2097152
